TPU v7x, 32 devices: a whole 2x2x4 slice. The times are simulated.
32 devices in a mesh: sp: 4 (over y, x), tp: 8 (over z, core).
Axes of the slice: x: 2, y: 2, z: 4, core: 2. Of those that a mesh axis runs over, the one named last changes fastest.
Arguments:
- latent: bfloat16 [2048, 4096], P(('sp', 'tp')), may hold values from -6 to 6
- context: bfloat16 [512, 4096], P('sp'), may hold values from -6 to 6
- condition: float32 [4096], replicated, may hold values from -6 to 6
- context_condition: float32 [4096], replicated, may hold values from -6 to 6
- modulation: bfloat16 [3, 4096, 4096], P(None, 'sp', 'tp'), may hold values from -0.09375 to 0.09375
- query_weight: bfloat16 [4096, 4096], P(None, 'tp'), as said below
- key_weight: bfloat16 [4096, 4096], P(None, 'tp'), as said below
- value_weight: bfloat16 [4096, 4096], P(None, 'tp'), may hold values from -0.09375 to 0.09375
- lambdas: float32 [16], P('tp'), may hold values from 0.3 to 0.8
- context_lift: float32 [16], P('tp'), may hold values from 1.5 to 3
- head_gain: float32 [256], replicated, may hold values from 0.1 to 1.9
- output_weight: bfloat16 [4096, 4096], P('tp'), may hold values from -0.09375 to 0.09375
Outputs:
- result: bfloat16 [2048, 4096], P(('sp', 'tp'))
Inputs may be any that keep to these rules, and one draw needn't show every extreme that they name: `query_weight`: entries lie within 200 / sqrt(4096) in magnitude. `key_weight`: entries lie within 6 / sqrt(4096) in magnitude.
All inputs are finite; a program needn't handle non-finite values.
Results may differ from a plain program's by a relative error of at most 0.025.
Values may be sent and summed in bfloat16 or wider, within the bound.
A program may use at most 64 MiB of HBM per device.

v0:
```python
import math
import jax
import jax.numpy as jnp
from jax import lax
from jax.sharding import PartitionSpec as P

GRID_W = 64
ROPE_BASE = 10000.0
EPSILON = 1e-05


def modulate(tokens_in, offset, scaling):
    values = tokens_in.astype(jnp.float32)
    center = jnp.mean(values, axis=-1, keepdims=True)
    spread = jnp.mean(jnp.square(values - center), axis=-1, keepdims=True)
    normed = (values - center) * lax.rsqrt(spread + EPSILON)
    return (normed * (1.0 + scaling) + offset).astype(jnp.bfloat16)


def rotate(tensor, places):
    number, head_count, head_width = tensor.shape
    quarter = head_width // 4
    eighth = head_width // 8
    inverse = ROPE_BASE ** (-jnp.arange(eighth, dtype=jnp.float32) / eighth)
    grid_row = (places // GRID_W).astype(jnp.float32)
    grid_col = (places % GRID_W).astype(jnp.float32)
    angles = jnp.stack([grid_row[:, None] * inverse, grid_col[:, None] * inverse], axis=1)
    cosine = jnp.cos(angles)[:, None, None, :, :]
    sine_table = jnp.sin(angles)[:, None, None, :, :]
    pieces = tensor.reshape(number, head_count, 2, 2, quarter)
    first_half = pieces[..., :eighth]
    second = pieces[..., eighth:]
    turned = jnp.concatenate(
        [first_half * cosine - second * sine_table, second * cosine + first_half * sine_table],
        axis=-1,
    )
    return turned.reshape(number, head_count, head_width)


def absorb(state_in, key_block, queries, lift_term, scale_factor):
    running_max, running_sum, running_out = state_in
    key_count = key_block.shape[0]
    head_count = queries.shape[1]
    head_width = 2 * queries.shape[3]
    local_width = head_count * head_width
    key_part = key_block[:, :local_width].reshape(key_count, head_count, 2, head_width // 2)
    value_part = key_block[:, local_width:].reshape(key_count, head_count, head_width)
    scores = (
        jnp.einsum("qhmd,khmd->mqhk", queries, key_part, preferred_element_type=jnp.float32)
        * scale_factor
        + lift_term
    )
    new_max = jnp.maximum(running_max, jnp.max(scores, axis=-1))
    fading = jnp.exp(running_max - new_max)
    weights = jnp.exp(scores - new_max[..., None])
    new_sum = running_sum * fading + jnp.sum(weights, axis=-1)
    new_out = running_out * fading[..., None] + jnp.einsum(
        "mqhk,khd->mqhd",
        weights.astype(jnp.bfloat16),
        value_part,
        preferred_element_type=jnp.float32,
    )
    return (new_max, new_sum, new_out)


def shards(
    latent,
    context,
    condition,
    context_condition,
    modulation,
    query_weight,
    key_weight,
    value_weight,
    lambdas,
    context_lift,
    head_gain,
    output_weight,
):
    sp_index = lax.axis_index("sp")
    rows_block = modulation.shape[1]
    silu_pair = jax.nn.silu(jnp.stack([condition, context_condition])).astype(jnp.bfloat16)
    own_rows = lax.dynamic_slice_in_dim(silu_pair, sp_index * rows_block, rows_block, 1)
    partial_mod = jnp.einsum(
        "cd,rde->cre", own_rows, modulation, preferred_element_type=jnp.float32
    )
    summed = lax.psum(partial_mod, "sp")
    mod_vectors = lax.all_gather(summed, "tp", axis=2, tiled=True)
    head_count = lambdas.shape[0]
    head_width = query_weight.shape[1] // head_count
    half_width = head_width // 2
    local_width = head_count * head_width
    scale_factor = half_width ** (-0.5)
    normed = modulate(latent, mod_vectors[0, 0], mod_vectors[0, 1])
    projection = jnp.concatenate([query_weight, key_weight, value_weight], axis=1)
    projected = jnp.dot(
        lax.all_gather(normed, "tp", axis=0, tiled=True),
        projection,
        preferred_element_type=jnp.float32,
    ).astype(jnp.bfloat16)
    block_tokens = projected.shape[0]
    places = sp_index * block_tokens + jnp.arange(block_tokens, dtype=jnp.int32)
    queries = rotate(
        projected[:, :local_width]
        .astype(jnp.float32)
        .reshape(block_tokens, head_count, head_width),
        places,
    )
    queries = queries.astype(jnp.bfloat16).reshape(block_tokens, head_count, 2, half_width)
    latent_keys = rotate(
        projected[:, local_width : 2 * local_width]
        .astype(jnp.float32)
        .reshape(block_tokens, head_count, head_width),
        places,
    )
    latent_keys = latent_keys.astype(jnp.bfloat16).reshape(block_tokens, local_width)
    packed = jnp.concatenate([latent_keys, projected[:, 2 * local_width :]], axis=1)
    normed_context = modulate(context, mod_vectors[1, 0], mod_vectors[1, 1])
    own_context = jnp.dot(
        normed_context, projection[:, local_width:], preferred_element_type=jnp.float32
    ).astype(jnp.bfloat16)
    context_packed = lax.all_gather(own_context, "sp", axis=0, tiled=True)
    initial = (
        jnp.full((2, block_tokens, head_count), -jnp.inf, jnp.float32),
        jnp.zeros((2, block_tokens, head_count), jnp.float32),
        jnp.zeros((2, block_tokens, head_count, head_width), jnp.float32),
    )
    state_now = absorb(initial, context_packed, queries, context_lift[:, None], scale_factor)
    segment = lax.all_gather(packed, "sp", axis=0, tiled=True)
    length = segment.shape[0]
    block_len = math.gcd(length, 1024)
    stacked = segment.reshape(length // block_len, block_len, segment.shape[1])

    def one_block(state_step, block_rows):
        return (absorb(state_step, block_rows, queries, 0.0, scale_factor), None)

    running_max, running_sum, running_out = lax.scan(one_block, state_now, stacked)[0]
    means = running_out / running_sum[..., None]
    difference = means[0] - lambdas[None, :, None] * means[1]
    scaled = (
        difference
        * lax.rsqrt(jnp.mean(jnp.square(difference), axis=-1, keepdims=True) + EPSILON)
        * head_gain
    )
    attended = scaled.astype(jnp.bfloat16).reshape(block_tokens, local_width)
    mixture = lax.psum_scatter(
        jnp.dot(attended, output_weight, preferred_element_type=jnp.float32).astype(jnp.bfloat16),
        "tp",
        scatter_dimension=0,
        tiled=True,
    ).astype(jnp.float32)
    return (latent.astype(jnp.float32) + mod_vectors[0, 2] * mixture).astype(jnp.bfloat16)


def solution(mesh):
    in_specs = (
        P(("sp", "tp"), None),
        P("sp", None),
        P(),
        P(),
        P(None, "sp", "tp"),
        P(None, "tp"),
        P(None, "tp"),
        P(None, "tp"),
        P("tp"),
        P("tp"),
        P(),
        P("tp", None),
    )
    out_specs = P(("sp", "tp"), None)
    return jax.shard_map(shards, mesh=mesh, in_specs=in_specs, out_specs=out_specs, check_vma=False)
```

profile of v0, /device:TPU:0, one launch (start us, length us, event | category | flops | bytes accessed | tf_op | source)
XLA Modules:
  0.0 269.9 jit_solution(10086001366930255042)
XLA Ops:
  6.5 1.9 copy-done
  9.7 17.6 %psum.7 = f32[2,3,512]{2,0,1:T(2,128)S(1)} all-reduce(f32[2,3,512]{2,0,1:T(2,128)S(1)} %fusion.61), channel_id=1, replica_groups=mesh['sp'=4,'tp'=8] {'sp'}, use_global_device_ids=true, to_apply=%region_0.1 | all-reduce | flops 3072 | bytes 24576 | tf_op jit(solution)/shard_map/psum | solution.py:87
  27.3 14.1 %all_gather.12 = f32[2,3,4096]{2,0,1:T(2,128)S(1)} all-gather(f32[2,3,512]{2,0,1:T(2,128)S(1)} %psum.7), channel_id=1, replica_groups=mesh['sp'=4,'tp'=8] {'tp'}, dimensions={2}, use_global_device_ids=true | all-gather | bytes 110592 | tf_op jit(solution)/shard_map/all_gather | solution.py:88
  44.1 2.1 fusion.43
  48.2 5.0 %fusion.37 = bf16[128,1024]{1,0:T(8,128)(2,1)} fusion(bf16[4096,512]{1,0:T(8,128)(2,1)} %param.21, bf16[4096,512]{1,0:T(8,128)(2,1)} %param.20, bf16[128,4096]{1,0:T(8,128)(2,1)S(1)} %copy-done.3, f32[4096]{0:T(1024)S(1)} %bitcast.120, f32[4096]{0:T(1024)S(1)} %bitcast.121, f32[128]{0:T(128)S(1)} %add_rsqrt_fusion.2, f32[128]{0:T(128)S(1)} %broadcast_multiply_fusion.3), kind=kOutput, calls=%fused_computation.47 | convolution fusion | flops 1093795840 | bytes 9733120 | tf_op jit(solution)/shard_map/dot_general | solution.py:119
  54.5 37.9 %all-gather.6.cloned.1.call-done = bf16[512,4096]{1,0:T(8,128)(2,1)} async-done(((bf16[64,4096]{1,0:T(8,128)(2,1)}), bf16[512,4096]{1,0:T(8,128)(2,1)}) %all-gather.6.cloned.1.call-update) | async-done | bytes 4194320 | tf_op jit(solution)/shard_map/all_gather | solution.py:97
  92.4 12.5 %fusion.22 = bf16[512,1536]{1,0:T(8,128)(2,1)S(1)} fusion(bf16[512,4096]{1,0:T(8,128)(2,1)} %all-gather.6.cloned.1.call-done, bf16[4096,512]{1,0:T(8,128)(2,1)} %param.21, bf16[4096,512]{1,0:T(8,128)(2,1)} %param.20, bf16[4096,512]{1,0:T(8,128)(2,1)} %param.19), kind=kOutput, calls=%fused_computation.30 | convolution fusion | flops 6480986112 | bytes 18350080 | tf_op jit(solution)/shard_map/dot_general | solution.py:96
  106.7 2.0 subtract_convert_fusion
  110.5 9.1 %all-gather.4.cloned.1.call-done = bf16[512,1024]{1,0:T(8,128)(2,1)} async-done(((bf16[128,1024]{1,0:T(8,128)(2,1)}), bf16[512,1024]{1,0:T(8,128)(2,1)}) %all-gather.4.cloned.1.call-update) | async-done | bytes 1048592 | tf_op jit(solution)/shard_map/all_gather | solution.py:122
  125.1 2.0 bitcast_add_fusion.1
  127.1 46.9 %all-gather.8.cloned.1.call-done = bf16[2048,1024]{1,0:T(8,128)(2,1)} async-done(((bf16[512,1024]{1,0:T(8,128)(2,1)}), bf16[2048,1024]{1,0:T(8,128)(2,1)}) %all-gather.8.cloned.1.call-update) | async-done | bytes 4194320 | tf_op jit(solution)/shard_map/all_gather | solution.py:129
  174.0 28.7 %while.14 = (s32[]{:T(128)}, f32[2,512,2]{1,2,0:T(2,128)S(1)}, f32[2,512,2]{1,2,0:T(2,128)S(1)}, f32[2,512,2,256]{1,3,0,2:T(8,128)}, bf16[2,1024,1024]{2,1,0:T(8...) while((s32[]{:T(128)}, f32[2,512,2]{1,2,0:T(2,128)S(1)}, f32[2,512,2]{1,2,0:T(2,128)S(1)}, ...), condition=%wide.region_10.11_spmd, body=%wide.region_7.10_spmd.sunk | while | flops 1624248320 | bytes 44703824 | solution.py:137
  174.0 3.1 %constant_dynamic-slice_fusion.2 = bf16[1,1024,1024]{2,1,0:T(8,128)(2,1)} fusion(bf16[2,1024,1024]{2,1,0:T(8,128)(2,1)} %get-tuple-element.173, s32[]{:T(128)} %get-tuple-element.162), kind=kLoop, calls=%fused_computation.12.clone.1 | loop fusion | bytes 4194308 | tf_op jit(solution)/shard_map/while/body/jit(dynamic_index_in_dim)/dynamic_slice | solution.py:137
  177.1 2.9 %copy.75 = bf16[1,1024,1024]{1,2,0:T(8,128)(2,1)S(1)} copy(bf16[1,1024,1024]{2,1,0:T(8,128)(2,1)} %constant_dynamic-slice_fusion.2) | data formatting | bytes 4194304 | tf_op jit(solution)/shard_map/while/body/jit(dynamic_index_in_dim)/dynamic_slice | solution.py:137
  180.2 2.4 bitcast_reduce_fusion.3
  184.2 4.2 %bitcast_add_fusion.3 = f32[2,512,2,256]{1,3,0,2:T(8,128)} fusion(f32[2,512,2,256]{1,3,0,2:T(8,128)} %get-tuple-element.165, bf16[1024,2,256,1]{0,2,3,1:T(8,128)(2,1)S(1)} %bitcast.107, bf16[2,512,2,1024]{1,3,2,0:T(8,128)(2,1)S(1)} %get-tuple-element.153, f32[2,512,2]{1,0,2:T(2,128)S(1)} %copy.76), kind=kOutput, calls=%fused_computation.7.clone.1 | convolution fusion | flops 1074790400 | bytes 9445376 | tf_op jit(solution)/shard_map/while/body/eval_jaxpr/mqhk,khd->mqhd/dot_general | solution.py:57
  188.4 3.1 %constant_dynamic-slice_fusion.2 = bf16[1,1024,1024]{2,1,0:T(8,128)(2,1)} fusion(bf16[2,1024,1024]{2,1,0:T(8,128)(2,1)} %get-tuple-element.173, s32[]{:T(128)} %get-tuple-element.162), kind=kLoop, calls=%fused_computation.12.clone.1 | loop fusion | bytes 4194308 | tf_op jit(solution)/shard_map/while/body/jit(dynamic_index_in_dim)/dynamic_slice | solution.py:137
  191.5 2.9 %copy.75 = bf16[1,1024,1024]{1,2,0:T(8,128)(2,1)S(1)} copy(bf16[1,1024,1024]{2,1,0:T(8,128)(2,1)} %constant_dynamic-slice_fusion.2) | data formatting | bytes 4194304 | tf_op jit(solution)/shard_map/while/body/jit(dynamic_index_in_dim)/dynamic_slice | solution.py:137
  194.5 2.4 bitcast_reduce_fusion.3
  198.6 4.2 %bitcast_add_fusion.3 = f32[2,512,2,256]{1,3,0,2:T(8,128)} fusion(f32[2,512,2,256]{1,3,0,2:T(8,128)} %get-tuple-element.165, bf16[1024,2,256,1]{0,2,3,1:T(8,128)(2,1)S(1)} %bitcast.107, bf16[2,512,2,1024]{1,3,2,0:T(8,128)(2,1)S(1)} %get-tuple-element.153, f32[2,512,2]{1,0,2:T(2,128)S(1)} %copy.76), kind=kOutput, calls=%fused_computation.7.clone.1 | convolution fusion | flops 1074790400 | bytes 9445376 | tf_op jit(solution)/shard_map/while/body/eval_jaxpr/mqhk,khd->mqhd/dot_general | solution.py:57
  202.8 1.9 broadcast_divide_fusion
  206.8 4.3 %convolution_convert_fusion = bf16[512,4096]{1,0:T(8,128)(2,1)} fusion(bf16[512,512]{0,1:T(8,128)(2,1)S(1)} %fusion.50, bf16[512,4096]{1,0:T(8,128)(2,1)S(1)} %copy-done.2), kind=kOutput, calls=%fused_computation.23 | convolution fusion | flops 2149580800 | bytes 8912896 | tf_op jit(solution)/shard_map/dot_general | solution.py:147
  211.2 50.1 %reduce-scatter.2.cloned.1.call-done = bf16[64,4096]{1,0:T(8,128)(2,1)} async-done(((bf16[512,4096]{1,0:T(8,128)(2,1)}), bf16[64,4096]{1,0:T(8,128)(2,1)}) %reduce-scatter.2.cloned.1.call-update) | async-done | bytes 524304 | tf_op jit(solution)/shard_map/reduce_scatter | solution.py:146
  261.3 2.1 fusion.44
  (75 shorter events, 22.0 us)
Async XLA Ops:
  6.5 1.9 copy-start
  6.5 85.9 %all-gather.6.cloned.1.call-start = ((), (), s32[]{:S(2)}) async-start(), calls=%async_computation.2 | async-start | bytes 4718592 | tf_op jit(solution)/shard_map/all_gather | solution.py:97
  9.7 38.0 %copy-start.3 = (bf16[128,4096]{1,0:T(8,128)(2,1)S(1)}, bf16[128,4096]{1,0:T(8,128)(2,1)}, u32[]{:S(2)}) copy-start(bf16[128,4096]{1,0:T(8,128)(2,1)} %param.15) | copy-start | bytes 3145732
  46.2 73.4 %all-gather.4.cloned.1.call-start = ((), (), s32[]{:S(2)}) async-start(), calls=%async_computation.1 | async-start | bytes 1310720 | tf_op jit(solution)/shard_map/all_gather | solution.py:122
  53.2 120.9 %all-gather.8.cloned.1.call-start = ((), (), s32[]{:S(2)}) async-start(), calls=%async_computation.3 | async-start | bytes 5242880 | tf_op jit(solution)/shard_map/all_gather | solution.py:129
  106.7 2.3 copy-start.4
  108.7 1.7 copy-start.7
  108.7 1.8 copy-start.8
  108.8 12.4 %copy-start.5 = (bf16[512,2,2,2,32]{0,4,3,2,1:T(8,128)(2,1)S(1)}, bf16[512,2,2,2,32]{0,4,3,2,1:T(8,128)(2,1)}, u32[]{:S(2)}) copy-start(bf16[512,2,2,2,32]{0,4,3,2,1:T(8,128)(2,1)} %get-tuple-element.86) | copy-start | bytes 786436
  110.2 12.1 %copy-start.6 = (f32[2]{0:T(128)S(1)}, f32[2]{0:T(128)}, u32[]{:S(2)}) copy-start(f32[2]{0:T(128)} %param.23) | copy-start | bytes 28
  110.2 151.1 %reduce-scatter.2.cloned.1.call-start = ((), (), s32[]{:S(2)}) async-start(), calls=%async_computation.4 | async-start | bytes 4718592 | tf_op jit(solution)/shard_map/reduce_scatter | solution.py:146
  204.7 2.2 copy-start.2
  206.8 56.6 %copy-start.1 = (bf16[3,1024,512]{2,1,0:T(8,128)(2,1)S(1)}, bf16[3,1024,512]{2,1,0:T(8,128)(2,1)}, u32[]{:S(2)}) copy-start(bf16[3,1024,512]{2,1,0:T(8,128)(2,1)} %param.18) | copy-start | bytes 9437188
Sparse Core Ops, SparseCore 0:
  46.3 46.0 all-gather.5
  94.2 25.2 all-gather.3
  121.4 52.5 all-gather.7
  211.3 49.9 reduce-scatter.1
where the time goes:
time: 271 us; the launch traced here: 270 us
  waiting for transfers between devices  144 us (53%)
  matrix products  39.9 us (15%)
  blocking collectives  31.7 us (12%)
  other arithmetic  21.2 us (8%)
  local copies, waits for them, and re-layouts  19.3 us (7%)
  between operations  13.3 us (5%)
    reduce_scatter x1, waiting for transfers between devices, shards(): lax.psum_scatter(jnp.dot(attended, output_weight, preferred_element_type=...  50.1 us
    all_gather x1, waiting for transfers between devices, shards(): segment = lax.all_gather(packed, 'sp', axis=0, tiled=True)  46.9 us
    all_gather x1, waiting for transfers between devices, shards(): lax.all_gather(normed, 'tp', axis=0, tiled=True)  37.9 us
    psum x1, blocking collectives, shards(): summed = lax.psum(partial_mod, 'sp')  17.6 us
    all_gather x1, blocking collectives, shards(): mod_vectors = lax.all_gather(summed, 'tp', axis=2, tiled=True)  14.1 us
    dot_general x1, matrix products, shards(): jnp.dot(lax.all_gather(normed, 'tp', axis=0, tiled=True), projection, pre...  12.5 us
    dynamic_slice x4, local copies, waits for them, and re-layouts, shards(): lax.scan(one_block, state_now, stacked)[0]  11.9 us
    dot_general x3, matrix products, absorb(): jnp.einsum('mqhk,khd->mqhd', weights.astype(jnp.bfloat16), value_part, pr...  10.4 us
  transfers between devices with their start and end apart: 4, of which 4 were waited for; matrix products, arithmetic and copies ran while one was open for 12% of the time, Pallas kernels for 0%

commit v1 on v0

--- a/solution.py
+++ b/solution.py
@@ -3,6 +3,7 @@
 import jax.numpy as jnp
 from jax import lax
 from jax.sharding import PartitionSpec as P
+from jax.lax import all_gather
 
 GRID_W = 64
 ROPE_BASE = 10000.0
@@ -77,6 +78,10 @@
     head_gain,
     output_weight,
 ):
+
+    def launch_shelves(panel):
+        return all_gather(panel, "sp").sum(axis=0)
+
     sp_index = lax.axis_index("sp")
     rows_block = modulation.shape[1]
     silu_pair = jax.nn.silu(jnp.stack([condition, context_condition])).astype(jnp.bfloat16)
@@ -84,7 +89,7 @@
     partial_mod = jnp.einsum(
         "cd,rde->cre", own_rows, modulation, preferred_element_type=jnp.float32
     )
-    summed = lax.psum(partial_mod, "sp")
+    summed = launch_shelves(partial_mod)
     mod_vectors = lax.all_gather(summed, "tp", axis=2, tiled=True)
     head_count = lambdas.shape[0]
     head_width = query_weight.shape[1] // head_count

time: 271 us -> 264 us (0.974)
  blocking collectives: 31.7 us -> 24 us
    psum x1 -> x0, blocking collectives: 17.6 us -> none  [shards(): summed = lax.psum(partial_mod, 'sp')]
    all_gather x0 -> x1, blocking collectives: none -> 9.85 us  [launch_shelves(): return all_gather(panel, 'sp').sum(axis=0)]
  transfers between devices with their start and end apart: 4 -> 4, of which waited for: 4 -> 4; matrix products, arithmetic and copies ran while one was open for 12% -> 13% of each run, Pallas kernels for 0% -> 0%
where the time goes in v1:
time: 264 us; the launch traced here: 263 us
  waiting for transfers between devices  145 us (55%)
  matrix products  39.9 us (15%)
  blocking collectives  24 us (9%)
  other arithmetic  21.2 us (8%)
  local copies, waits for them, and re-layouts  19.3 us (7%)
  between operations  13.4 us (5%)
    reduce_scatter x1, waiting for transfers between devices, shards(): lax.psum_scatter(jnp.dot(attended, output_weight, preferred_element_type=...  50.1 us
    all_gather x1, waiting for transfers between devices, shards(): segment = lax.all_gather(packed, 'sp', axis=0, tiled=True)  46.9 us
    all_gather x1, waiting for transfers between devices, shards(): lax.all_gather(normed, 'tp', axis=0, tiled=True)  38.9 us
    all_gather x1, blocking collectives, shards(): mod_vectors = lax.all_gather(summed, 'tp', axis=2, tiled=True)  14.2 us
    dot_general x1, matrix products, shards(): jnp.dot(lax.all_gather(normed, 'tp', axis=0, tiled=True), projection, pre...  12.5 us
    dynamic_slice x4, local copies, waits for them, and re-layouts, shards(): lax.scan(one_block, state_now, stacked)[0]  11.9 us
    dot_general x3, matrix products, absorb(): jnp.einsum('mqhk,khd->mqhd', weights.astype(jnp.bfloat16), value_part, pr...  10.4 us
    all_gather x1, blocking collectives, launch_shelves(): return all_gather(panel, 'sp').sum(axis=0)  9.85 us
  transfers between devices with their start and end apart: 4, of which 4 were waited for; matrix products, arithmetic and copies ran while one was open for 13% of the time, Pallas kernels for 0%

profile of v1, /device:TPU:0, one launch (start us, length us, event | category | flops | bytes accessed | tf_op | source)
XLA Modules:
  0.0 263.2 jit_solution(8848866607551969156)
XLA Ops:
  6.5 1.9 copy-done
  9.7 9.8 %all-gather = f32[8,3,512]{2,1,0:T(4,128)S(1)} all-gather(f32[2,3,512]{2,1,0:T(4,128)S(1)} %copy.41), channel_id=2, replica_groups=mesh['sp'=4,'tp'=8] {'sp'}, dimensions={0}, use_global_device_ids=true | all-gather | bytes 61440 | tf_op jit(solution)/shard_map/all_gather | solution.py:83
  19.6 14.2 %all_gather.20 = f32[2,3,4096]{2,0,1:T(2,128)S(1)} all-gather(f32[2,3,512]{2,0,1:T(2,128)S(1)} %copy.67), channel_id=1, replica_groups=mesh['sp'=4,'tp'=8] {'tp'}, dimensions={2}, use_global_device_ids=true | all-gather | bytes 110592 | tf_op jit(solution)/shard_map/all_gather | solution.py:93
  36.4 2.1 fusion.43
  40.5 5.0 %fusion.37 = bf16[128,1024]{1,0:T(8,128)(2,1)} fusion(bf16[4096,512]{1,0:T(8,128)(2,1)} %param.21, bf16[4096,512]{1,0:T(8,128)(2,1)} %param.20, bf16[128,4096]{1,0:T(8,128)(2,1)S(1)} %copy-done.3, f32[4096]{0:T(1024)S(1)} %bitcast.122, f32[4096]{0:T(1024)S(1)} %bitcast.123, f32[128]{0:T(128)S(1)} %add_rsqrt_fusion.2, f32[128]{0:T(128)S(1)} %broadcast_multiply_fusion.3), kind=kOutput, calls=%fused_computation.47 | convolution fusion | flops 1093795840 | bytes 9733120 | tf_op jit(solution)/shard_map/dot_general | solution.py:124
  46.8 38.9 %all-gather.7.cloned.1.call-done = bf16[512,4096]{1,0:T(8,128)(2,1)} async-done(((bf16[64,4096]{1,0:T(8,128)(2,1)}), bf16[512,4096]{1,0:T(8,128)(2,1)}) %all-gather.7.cloned.1.call-update) | async-done | bytes 4194320 | tf_op jit(solution)/shard_map/all_gather | solution.py:102
  85.7 12.5 %fusion.22 = bf16[512,1536]{1,0:T(8,128)(2,1)S(1)} fusion(bf16[512,4096]{1,0:T(8,128)(2,1)} %all-gather.7.cloned.1.call-done, bf16[4096,512]{1,0:T(8,128)(2,1)} %param.21, bf16[4096,512]{1,0:T(8,128)(2,1)} %param.20, bf16[4096,512]{1,0:T(8,128)(2,1)} %param.19), kind=kOutput, calls=%fused_computation.30 | convolution fusion | flops 6480986112 | bytes 18350080 | tf_op jit(solution)/shard_map/dot_general | solution.py:101
  100.0 2.0 subtract_convert_fusion
  103.8 9.1 %all-gather.5.cloned.1.call-done = bf16[512,1024]{1,0:T(8,128)(2,1)} async-done(((bf16[128,1024]{1,0:T(8,128)(2,1)}), bf16[512,1024]{1,0:T(8,128)(2,1)}) %all-gather.5.cloned.1.call-update) | async-done | bytes 1048592 | tf_op jit(solution)/shard_map/all_gather | solution.py:127
  118.3 2.0 bitcast_add_fusion.1
  120.4 46.9 %all-gather.9.cloned.1.call-done = bf16[2048,1024]{1,0:T(8,128)(2,1)} async-done(((bf16[512,1024]{1,0:T(8,128)(2,1)}), bf16[2048,1024]{1,0:T(8,128)(2,1)}) %all-gather.9.cloned.1.call-update) | async-done | bytes 4194320 | tf_op jit(solution)/shard_map/all_gather | solution.py:134
  167.3 28.7 %while.14 = (s32[]{:T(128)}, f32[2,512,2]{1,2,0:T(2,128)S(1)}, f32[2,512,2]{1,2,0:T(2,128)S(1)}, f32[2,512,2,256]{1,3,0,2:T(8,128)}, bf16[2,1024,1024]{2,1,0:T(8...) while((s32[]{:T(128)}, f32[2,512,2]{1,2,0:T(2,128)S(1)}, f32[2,512,2]{1,2,0:T(2,128)S(1)}, ...), condition=%wide.region_10.11_spmd, body=%wide.region_7.10_spmd.sunk | while | flops 1624248320 | bytes 44703824 | solution.py:142
  167.3 3.1 %constant_dynamic-slice_fusion.2 = bf16[1,1024,1024]{2,1,0:T(8,128)(2,1)} fusion(bf16[2,1024,1024]{2,1,0:T(8,128)(2,1)} %get-tuple-element.179, s32[]{:T(128)} %get-tuple-element.168), kind=kLoop, calls=%fused_computation.12.clone.1 | loop fusion | bytes 4194308 | tf_op jit(solution)/shard_map/while/body/jit(dynamic_index_in_dim)/dynamic_slice | solution.py:142
  170.4 2.9 %copy.93 = bf16[1,1024,1024]{1,2,0:T(8,128)(2,1)S(1)} copy(bf16[1,1024,1024]{2,1,0:T(8,128)(2,1)} %constant_dynamic-slice_fusion.2) | data formatting | bytes 4194304 | tf_op jit(solution)/shard_map/while/body/jit(dynamic_index_in_dim)/dynamic_slice | solution.py:142
  173.4 2.4 bitcast_reduce_fusion.3
  177.5 4.2 %bitcast_add_fusion.3 = f32[2,512,2,256]{1,3,0,2:T(8,128)} fusion(f32[2,512,2,256]{1,3,0,2:T(8,128)} %get-tuple-element.171, bf16[1024,2,256,1]{0,2,3,1:T(8,128)(2,1)S(1)} %bitcast.108, bf16[2,512,2,1024]{1,3,2,0:T(8,128)(2,1)S(1)} %get-tuple-element.159, f32[2,512,2]{1,0,2:T(2,128)S(1)} %copy.94), kind=kOutput, calls=%fused_computation.7.clone.1 | convolution fusion | flops 1074790400 | bytes 9445376 | tf_op jit(solution)/shard_map/while/body/eval_jaxpr/mqhk,khd->mqhd/dot_general | solution.py:58
  181.6 3.1 %constant_dynamic-slice_fusion.2 = bf16[1,1024,1024]{2,1,0:T(8,128)(2,1)} fusion(bf16[2,1024,1024]{2,1,0:T(8,128)(2,1)} %get-tuple-element.179, s32[]{:T(128)} %get-tuple-element.168), kind=kLoop, calls=%fused_computation.12.clone.1 | loop fusion | bytes 4194308 | tf_op jit(solution)/shard_map/while/body/jit(dynamic_index_in_dim)/dynamic_slice | solution.py:142
  184.7 2.9 %copy.93 = bf16[1,1024,1024]{1,2,0:T(8,128)(2,1)S(1)} copy(bf16[1,1024,1024]{2,1,0:T(8,128)(2,1)} %constant_dynamic-slice_fusion.2) | data formatting | bytes 4194304 | tf_op jit(solution)/shard_map/while/body/jit(dynamic_index_in_dim)/dynamic_slice | solution.py:142
  187.8 2.4 bitcast_reduce_fusion.3
  191.8 4.2 %bitcast_add_fusion.3 = f32[2,512,2,256]{1,3,0,2:T(8,128)} fusion(f32[2,512,2,256]{1,3,0,2:T(8,128)} %get-tuple-element.171, bf16[1024,2,256,1]{0,2,3,1:T(8,128)(2,1)S(1)} %bitcast.108, bf16[2,512,2,1024]{1,3,2,0:T(8,128)(2,1)S(1)} %get-tuple-element.159, f32[2,512,2]{1,0,2:T(2,128)S(1)} %copy.94), kind=kOutput, calls=%fused_computation.7.clone.1 | convolution fusion | flops 1074790400 | bytes 9445376 | tf_op jit(solution)/shard_map/while/body/eval_jaxpr/mqhk,khd->mqhd/dot_general | solution.py:58
  196.0 1.9 broadcast_divide_fusion
  200.1 4.3 %convolution_convert_fusion = bf16[512,4096]{1,0:T(8,128)(2,1)} fusion(bf16[512,512]{0,1:T(8,128)(2,1)S(1)} %fusion.50, bf16[512,4096]{1,0:T(8,128)(2,1)S(1)} %copy-done.2), kind=kOutput, calls=%fused_computation.23 | convolution fusion | flops 2149580800 | bytes 8912896 | tf_op jit(solution)/shard_map/dot_general | solution.py:152
  204.4 50.1 %reduce-scatter.2.cloned.1.call-done = bf16[64,4096]{1,0:T(8,128)(2,1)} async-done(((bf16[512,4096]{1,0:T(8,128)(2,1)}), bf16[64,4096]{1,0:T(8,128)(2,1)}) %reduce-scatter.2.cloned.1.call-update) | async-done | bytes 524304 | tf_op jit(solution)/shard_map/reduce_scatter | solution.py:151
  254.5 2.1 fusion.44
  (78 shorter events, 22.0 us)
Async XLA Ops:
  6.5 1.9 copy-start
  6.5 79.1 %all-gather.7.cloned.1.call-start = ((), (), s32[]{:S(2)}) async-start(), calls=%async_computation.2 | async-start | bytes 4718592 | tf_op jit(solution)/shard_map/all_gather | solution.py:102
  9.7 30.4 %copy-start.3 = (bf16[128,4096]{1,0:T(8,128)(2,1)S(1)}, bf16[128,4096]{1,0:T(8,128)(2,1)}, u32[]{:S(2)}) copy-start(bf16[128,4096]{1,0:T(8,128)(2,1)} %param.15) | copy-start | bytes 3145732
  38.5 74.3 %all-gather.5.cloned.1.call-start = ((), (), s32[]{:S(2)}) async-start(), calls=%async_computation.1 | async-start | bytes 1310720 | tf_op jit(solution)/shard_map/all_gather | solution.py:127
  45.5 121.8 %all-gather.9.cloned.1.call-start = ((), (), s32[]{:S(2)}) async-start(), calls=%async_computation.3 | async-start | bytes 5242880 | tf_op jit(solution)/shard_map/all_gather | solution.py:134
  99.9 2.3 copy-start.4
  102.0 1.7 copy-start.7
  102.0 1.8 copy-start.8
  102.0 12.4 %copy-start.5 = (bf16[512,2,2,2,32]{0,4,3,2,1:T(8,128)(2,1)S(1)}, bf16[512,2,2,2,32]{0,4,3,2,1:T(8,128)(2,1)}, u32[]{:S(2)}) copy-start(bf16[512,2,2,2,32]{0,4,3,2,1:T(8,128)(2,1)} %get-tuple-element.92) | copy-start | bytes 786436
  103.4 12.1 %copy-start.6 = (f32[2]{0:T(128)S(1)}, f32[2]{0:T(128)}, u32[]{:S(2)}) copy-start(f32[2]{0:T(128)} %param.23) | copy-start | bytes 28
  103.4 151.1 %reduce-scatter.2.cloned.1.call-start = ((), (), s32[]{:S(2)}) async-start(), calls=%async_computation.4 | async-start | bytes 4718592 | tf_op jit(solution)/shard_map/reduce_scatter | solution.py:151
  197.9 2.2 copy-start.2
  200.1 56.6 %copy-start.1 = (bf16[3,1024,512]{2,1,0:T(8,128)(2,1)S(1)}, bf16[3,1024,512]{2,1,0:T(8,128)(2,1)}, u32[]{:S(2)}) copy-start(bf16[3,1024,512]{2,1,0:T(8,128)(2,1)} %param.18) | copy-start | bytes 9437188
Sparse Core Ops, SparseCore 0:
  38.7 46.9 all-gather.6
  87.5 25.2 all-gather.4
  114.7 52.5 all-gather.8
  204.6 49.9 reduce-scatter.1
